TPU v7x, 32 devices: a whole 2x2x4 slice. The times are simulated.
32 devices in a mesh: sp: 16 (over z, y, core), tp: 2 (over x).
Axes of the slice: x: 2, y: 2, z: 4, core: 2. Of those that a mesh axis runs over, the one named last changes fastest.
Arguments:
- incoming_activity: bfloat16 [8192, 2048], P(('sp', 'tp')), may hold values from -6 to 6
- entry_standardize_factor: bfloat16 [2048], replicated, may hold values from 0.099609375 to 1.8984375
- recursive_entry_matrix: bfloat16 [2048, 2048], P(None, 'tp'), may hold values from -0.125 to 0.125
- final_switch_matrix: bfloat16 [2048, 2048], P(None, 'tp'), may hold values from -0.125 to 0.125
- averaging_entry_matrix: bfloat16 [2048, 1024], P(None, 'tp'), may hold values from -0.125 to 0.125
- percolumn_filter_coefficients: bfloat16 [4, 2048], P(None, 'tp'), may hold values from -3 to 3
- switch_tiled_matrices: bfloat16 [2, 2, 32, 64, 64], P(None, None, 'tp'), may hold values from -0.75 to 0.75
- prior_fading_odds: float32 [2, 2048], P(None, 'tp'), may hold values from 2.7 to 17
- speed_factors: float32 [2, 8192], P(None, 'sp'), may hold values from 0.4 to 2.5, as said below
- extra_fading_amounts: float32 [2, 8192], P(None, 'sp'), may hold values from -1.39 to 0, as said below
- averaging_cluster_matrices: bfloat16 [8, 128, 128], P('tp'), may hold values from -0.5 to 0.5
- averaging_feature_factor: bfloat16 [1024], P('tp'), may hold values from 0.099609375 to 1.8984375
- recursive_final_matrix: bfloat16 [2048, 2048], P('tp'), may hold values from -0.25 to 0.25
- averaging_final_matrix: bfloat16 [1024, 2048], P('tp'), may hold values from -0.1875 to 0.1875
Outputs:
- mixed: bfloat16 [8192, 2048], P(('sp', 'tp'))
Inputs may be any that keep to these rules, and one draw needn't show every extreme that they name: `speed_factors`: constant over each aligned block of 512 positions. `extra_fading_amounts`: each row has at most two nonzero entries.
All inputs are finite; a program needn't handle non-finite values.
Results may differ from a plain program's by a relative error of at most 0.017.
Values may be sent and summed in bfloat16 or wider, within the bound.
A program may use at most 128 MiB of HBM per device.

v0:
```python
import jax
import jax.numpy as jnp
from jax import lax
from jax.sharding import PartitionSpec as P

FADING_FACTOR = 8.0
epsilon = 1e-06
span_rows = 16


def padded(block, sides, width):
    for axis, dim in sides:
        count = lax.axis_size(axis)
        forward = [(i, i + 1) for i in range(count - 1)]
        backward = [(target, source) for source, target in forward]
        low = lax.ppermute(
            lax.slice_in_dim(block, block.shape[dim] - width, None, axis=dim), axis, forward
        )
        high = lax.ppermute(lax.slice_in_dim(block, 0, width, axis=dim), axis, backward)
        block = jnp.concatenate([low, block, high], axis=dim)
    return block


def combine(earlier, later):
    return (earlier[0] * later[0], later[0] * earlier[1] + later[1])


def product(left, right):
    return jnp.dot(left, right, preferred_element_type=jnp.float32)


def block_chain(log_keep, drive, backward):
    length, width = log_keep.shape
    count = length // span_rows
    logs = log_keep.reshape(count, span_rows, width)
    sources = drive.reshape(count, span_rows, width)
    running = jnp.cumsum(logs, axis=1)
    place = jnp.arange(span_rows, dtype=jnp.int32)
    if backward:
        running = running[:, -1:] - running + logs
        inside = place[None, :] >= place[:, None]
    else:
        inside = place[None, :] <= place[:, None]
    inside = inside[None, :, :, None]
    spread = running[:, :, None, :] - running[:, None, :, :]
    weights = jnp.where(inside, jnp.exp(jnp.where(inside, spread, 0.0)), 0.0)
    within = jnp.einsum("btsc,bsc->btc", weights, sources)
    decay = jnp.exp(running)
    ones = jnp.ones((1, width), jnp.float32)
    zeros = jnp.zeros((1, width), jnp.float32)
    if backward:
        ends = (decay[:, 0], within[:, 0])
        total_keep, total_state = lax.associative_scan(combine, ends, axis=0, reverse=True)
        prior_keep = jnp.concatenate([total_keep[1:], ones], axis=0)
        prior_state = jnp.concatenate([total_state[1:], zeros], axis=0)
    else:
        ends = (decay[:, -1], within[:, -1])
        total_keep, total_state = lax.associative_scan(combine, ends, axis=0)
        prior_keep = jnp.concatenate([ones, total_keep[:-1]], axis=0)
        prior_state = jnp.concatenate([zeros, total_state[:-1]], axis=0)
    keep_all = decay * prior_keep[:, None]
    local_all = within + decay * prior_state[:, None]
    return (keep_all.reshape(length, width), local_all.reshape(length, width))


def local(
    incoming_activity,
    entry_standardize_factor,
    recursive_entry_matrix,
    final_switch_matrix,
    averaging_entry_matrix,
    percolumn_filter_coefficients,
    switch_tiled_matrices,
    prior_fading_odds,
    speed_factors,
    extra_fading_amounts,
    averaging_cluster_matrices,
    averaging_feature_factor,
    recursive_final_matrix,
    averaging_final_matrix,
):
    state_width = recursive_entry_matrix.shape[1]
    pool_width = averaging_entry_matrix.shape[1]
    gain = entry_standardize_factor.astype(jnp.float32)
    values = lax.all_gather(incoming_activity, "tp", axis=0, tiled=True).astype(jnp.float32)
    scaled = values * lax.rsqrt(jnp.mean(values * values, axis=1, keepdims=True) + epsilon)
    normed = (scaled * gain).astype(jnp.bfloat16)
    projected = jnp.concatenate(
        [
            product(normed, weight).astype(jnp.bfloat16)
            for weight in (recursive_entry_matrix, final_switch_matrix, averaging_entry_matrix)
        ],
        axis=1,
    )
    length = projected.shape[0]
    state_input = projected[:, :state_width]
    gate_input = projected[:, state_width : 2 * state_width]
    pool_input = projected[:, 2 * state_width :]
    conv_rows = padded(state_input, (("sp", 0),), 2).astype(jnp.float32)
    filtered = percolumn_filter_coefficients[0].astype(jnp.float32) * conv_rows[0:length]
    for shift in range(1, percolumn_filter_coefficients.shape[0]):
        filtered = (
            filtered
            + percolumn_filter_coefficients[shift].astype(jnp.float32)
            * conv_rows[shift : shift + length]
        )
    filtered = filtered.astype(jnp.bfloat16)
    filtered_wide = filtered.astype(jnp.float32)
    blocks_here = switch_tiled_matrices.shape[2]
    block_width = switch_tiled_matrices.shape[3]
    gate_sums = jnp.einsum(
        "tbi,dqbij->tdqbj",
        filtered.reshape(length, blocks_here, block_width),
        switch_tiled_matrices,
        preferred_element_type=jnp.float32,
    ).reshape(length, 2, 2, state_width)
    remember_switch = jax.nn.sigmoid(gate_sums[:, :, 0])
    inlet = jax.nn.sigmoid(gate_sums[:, :, 1])
    fading_speed = jax.nn.softplus(-prior_fading_odds)
    logarithmic_persistence = (
        -FADING_FACTOR
        * jnp.transpose(speed_factors)[:, :, None]
        * remember_switch
        * fading_speed[None]
        + jnp.transpose(extra_fading_amounts)[:, :, None]
    )
    drive = jnp.sqrt(-jnp.expm1(2.0 * logarithmic_persistence)) * inlet * filtered_wide[:, None, :]
    forward_keep, forward_local = block_chain(logarithmic_persistence[:, 0], drive[:, 0], False)
    backward_keep, backward_local = block_chain(logarithmic_persistence[:, 1], drive[:, 1], True)
    zeros = jnp.zeros((state_width,), jnp.float32)
    summary = jnp.stack([forward_keep[-1], forward_local[-1], backward_keep[0], backward_local[0]])[
        None
    ]
    totals = lax.all_gather(summary, "sp", axis=0, tiled=True)
    place = lax.axis_index("sp")
    forward_all = lax.associative_scan(combine, (totals[:, 0], totals[:, 1]), axis=0)
    backward_all = lax.associative_scan(combine, (totals[:, 2], totals[:, 3]), axis=0, reverse=True)
    forward_before = jnp.concatenate([zeros[None], forward_all[1]], axis=0)
    backward_after = jnp.concatenate([backward_all[1], zeros[None]], axis=0)
    forward_carry = lax.dynamic_index_in_dim(forward_before, place, 0, keepdims=False)
    backward_carry = lax.dynamic_index_in_dim(backward_after, place + 1, 0, keepdims=False)
    state_sum = (
        forward_local
        + forward_keep * forward_carry[None]
        + backward_local
        + backward_keep * backward_carry[None]
    )
    state_mix = (jax.nn.gelu(gate_input.astype(jnp.float32)) * state_sum).astype(jnp.bfloat16)
    pool_rows = padded(pool_input, (("sp", 0),), 8).astype(jnp.float32)
    spans = []
    level = pool_rows
    for step in range(4):
        shift = 1 << step
        level = level[:-shift] + level[shift:]
        spans.append(level)
    group_width = averaging_cluster_matrices.shape[1]
    local_groups = pool_width // group_width
    group_index = (
        lax.axis_index("tp") * local_groups + jnp.arange(pool_width, dtype=jnp.int32) // group_width
    )
    window_code = group_index % 4
    position = lax.axis_index("sp") * length + jnp.arange(length, dtype=jnp.int32)
    total_length = length * lax.axis_size("sp")
    window_sum = jnp.zeros((length, pool_width), jnp.float32)
    counted = jnp.ones((length, pool_width), jnp.float32)
    for code in range(4):
        half = 1 << code
        begin = 8 - half
        chosen = (window_code == code)[None, :]
        window_count = (
            jnp.minimum(position + half, total_length) - jnp.maximum(position - half, 0)
        ).astype(jnp.float32)[:, None]
        window_sum = jnp.where(chosen, spans[code][begin : begin + length], window_sum)
        counted = jnp.where(chosen, window_count, counted)
    pooled = (window_sum / counted - pool_rows[8 : 8 + length]).astype(jnp.bfloat16)
    grouped = jnp.einsum(
        "tgi,gij->tgj",
        pooled.reshape(length, local_groups, group_width),
        averaging_cluster_matrices,
        preferred_element_type=jnp.float32,
    ).reshape(length, pool_width)
    pool_mix = (grouped * averaging_feature_factor.astype(jnp.float32)).astype(jnp.bfloat16)
    return lax.psum_scatter(
        (
            product(state_mix, recursive_final_matrix) + product(pool_mix, averaging_final_matrix)
        ).astype(jnp.bfloat16),
        "tp",
        scatter_dimension=0,
        tiled=True,
    )


def solution(mesh):
    in_specs = (
        P(("sp", "tp"), None),
        P(),
        P(None, "tp"),
        P(None, "tp"),
        P(None, "tp"),
        P(None, "tp"),
        P(None, None, "tp", None, None),
        P(None, "tp"),
        P(None, "sp"),
        P(None, "sp"),
        P("tp", None, None),
        P("tp"),
        P("tp", None),
        P("tp", None),
    )
    out_specs = P(("sp", "tp"), None)
    return jax.shard_map(local, mesh=mesh, in_specs=in_specs, out_specs=out_specs, check_vma=False)
```

profile of v0, /device:TPU:0, one launch (start us, length us, event | category | flops | bytes accessed | tf_op | source)
XLA Modules:
  0.0 251.2 jit_solution(8073936475268317214)
XLA Ops:
  6.6 0.7 all-gather.4.cloned.1.call-update
  7.3 0.7 convert_element_type.101
  8.0 0.7 convert_element_type.85
  8.7 1.6 copy.54
  10.5 34.2 %all-gather.4.cloned.1.call-done = bf16[512,2048]{1,0:T(8,128)(2,1)} async-done(((bf16[256,2048]{1,0:T(8,128)(2,1)}), bf16[512,2048]{1,0:T(8,128)(2,1)}) %all-gather.4.cloned.1.call-update) | async-done | bytes 2097168 | tf_op jit(solution)/shard_map/all_gather | solution.py:85
  44.7 2.2 fusion
  47.0 4.7 %convolution_convert_fusion = bf16[512,1024]{1,0:T(8,128)(2,1)S(1)} fusion(bf16[2048,1024]{1,0:T(8,128)(2,1)} %param.16, bf16[512,2048]{1,0:T(8,128)(2,1)S(1)} %copy-done.9, f32[2048]{0:T(1024)S(1)} %convert_element_type.85, f32[512]{0:T(512)S(1)} %add_rsqrt_fusion), kind=kOutput, calls=%fused_computation.44 | convolution fusion | flops 2152202240 | bytes 7350272 | tf_op jit(solution)/shard_map/dot_general | solution.py:29
  51.8 1.6 collective-permute-start
  53.3 1.3 collective-permute-start.1
  54.6 1.3 convolution_convert_fusion.2
  56.0 4.5 %collective-permute-start.2 = (bf16[8,512]{1,0:T(8,128)(2,1)S(1)}, bf16[8,512]{1,0:T(8,128)(2,1)S(1)}, u32[]{:S(2)}, u32[]{:S(2)}) collective-permute-start(bf16[8,512]{1,0:T(8,128)(2,1)S(1)} %get-tuple-element.24), channel_id=1, source_target_pairs={{0,2},{2,4},{4,6},{6,8},{8,10},{10,12},{12,14},{14,16},{16,18},{18... | collective-permute-start | bytes 24584 | tf_op jit(solution)/shard_map/ppermute | solution.py:16
  60.4 1.3 collective-permute-start.3
  61.8 0.3 maximum_convert_fusion
  62.1 2.6 %fusion.71 = (f32[512,1024]{1,0:T(8,128)}, bf16[512,1024]{1,0:T(8,128)(2,1)}) fusion(f32[516,1024]{1,0:T(8,128)S(1)} %maximum_convert_fusion, f32[1024]{0:T(1024)S(1)} %bitcast.154, f32[1024]{0:T(1024)S(1)} %bitcast.155, f32[1024]{0:T(1024)S(1)} %bitcast.153, f32[1024]{0:T(1024)S(1)} %bitcast.152), kind=kLoop, calls=%fused_computation.227 | loop fusion | flops 4718592 | bytes 11550720 | tf_op jit(solution)/shard_map/convert_element_type | solution.py:108
  64.7 2.8 %copy.53 = bf16[512,1024]{0,1:T(8,128)(2,1)} copy(bf16[512,1024]{1,0:T(8,128)(2,1)} %get-tuple-element.8) | data formatting | bytes 2097152 | tf_op jit(solution)/shard_map/convert_element_type | solution.py:107
  67.4 2.5 fusion.96
  69.9 1.8 copy.55
  71.7 4.2 %fusion.74 = (f32[512,2,1,1024]{0,3,2,1:T(8,128)}, f32[512,2,1,1024]{0,3,2,1:T(8,128)}) fusion(f32[512,2,2,1024]{0,3,2,1:T(8,128)S(1)} %bitcast.122), kind=kLoop, calls=%fused_computation.229 | loop fusion | bytes 16777216 | tf_op jit(solution)/shard_map/slice | solution.py:117
  75.9 5.4 %copy.92 = f32[512,2,1,1024]{3,0,1,2:T(8,128)} copy(f32[512,2,1,1024]{0,3,2,1:T(8,128)} %get-tuple-element.12) | data formatting | bytes 8388608
  81.3 5.4 %copy.93 = f32[512,2,1,1024]{3,0,1,2:T(8,128)} copy(f32[512,2,1,1024]{0,3,2,1:T(8,128)} %get-tuple-element.13) | data formatting | bytes 8388608
  86.7 7.3 %fusion.3 = (f32[512,2,1024]{2,0,1:T(8,128)S(1)}, f32[512,2,1024]{2,0,1:T(8,128)S(1)}) fusion(f32[512,2,1,1024]{3,0,1,2:T(8,128)} %copy.93, f32[512,1024]{1,0:T(8,128)} %get-tuple-element.7, f32[512,2]{0,1:T(2,128)S(1)} %bitcast.158, f32[2,1024]{1,0:T(2,128)S(1)} %compare_select_fusion, f32[512,2,1,1024]{3,0,1,2:T(8,128)} %copy.92, ...), kind=kLoop, calls=%fused_computation.8 | loop fusion | flops 13631488 | bytes 18890752 | tf_op jit(solution)/shard_map/mul | solution.py:127
  94.0 3.3 %fusion.75 = (f32[512,1,1024]{2,0,1:T(8,128)}, f32[512,1,1024]{2,0,1:T(8,128)S(1)}, f32[512,1,1024]{2,0,1:T(8,128)}, f32[512,1,1024]{2,0,1:T(8,128)}) fusion(f32[512,2,1024]{2,0,1:T(8,128)S(1)} %get-tuple-element.6, f32[512,2,1024]{2,0,1:T(8,128)S(1)} %get-tuple-element.5), kind=kLoop, calls=%fused_computation.230 | loop fusion | bytes 16777216 | tf_op jit(solution)/shard_map/slice | solution.py:128
  97.3 0.6 copy-done.1
  97.9 1.3 fusion.20
  99.2 3.6 %fusion.73 = (f32[32,16,1024]{2,0,1:T(8,128)S(1)}, f32[32,16,1024]{2,0,1:T(8,128)}, f32[32,16,1024]{2,0,1:T(8,128)}) fusion(f32[32,16,1024]{2,1,0:T(8,128)S(1)} %bitcast.124, f32[32,16,1024]{2,0,1:T(8,128)S(1)} %fusion.20, f32[32,1024]{1,0:T(8,128)S(1)} %slice_bitcast_fusion.2), kind=kLoop, calls=%fused_computation.228 | loop fusion | flops 1048576 | bytes 10616832 | tf_op jit(solution)/shard_map/exp | solution.py:48
  102.9 3.0 %copy.66 = f32[32,16,1024]{2,1,0:T(8,128)S(1)} copy(f32[32,16,1024]{2,0,1:T(8,128)} %get-tuple-element.10) | data formatting | bytes 4194304 | tf_op jit(solution)/shard_map/add | solution.py:40
  105.9 12.3 %multiply_reduce_fusion = f32[32,1024,16]{1,2,0:T(8,128)S(1)} fusion(f32[32,1024,16]{1,2,0:T(8,128)S(1)} %bitcast.139, f32[32,16,1024]{2,1,0:T(8,128)S(1)} %copy.66, pred[16,16]{1,0:T(8,128)(4,1)S(1)} %iota_compare_fusion), kind=kLoop, calls=%fused_computation | loop fusion | flops 41418752 | bytes 6291712
  118.2 1.2 copy.121
  119.6 0.2 slice.739
  119.8 0.2 slice.741
  119.9 0.2 slice.770
  120.1 0.2 slice.772
  120.9 4.3 %fusion.95 = (f32[32,16,1024]{2,0,1:T(8,128)S(1)}, f32[32,16,1024]{2,0,1:T(8,128)}) fusion(f32[32,16,1024]{2,1,0:T(8,128)} %bitcast.125), kind=kOutput, calls=%fused_computation.250 | output fusion | flops 7864320 | bytes 6291456 | tf_op jit(solution)/shard_map/jit(cumsum)/reduce_window_sum | solution.py:37
  125.3 3.0 %copy.59 = f32[32,16,1024]{2,1,0:T(8,128)S(1)} copy(f32[32,16,1024]{2,0,1:T(8,128)} %get-tuple-element.97) | data formatting | bytes 4194304 | tf_op jit(solution)/shard_map/jit(cumsum)/reduce_window_sum | solution.py:37
  128.3 12.1 %multiply_reduce_fusion.1 = f32[32,1024,16]{1,2,0:T(8,128)S(1)} fusion(f32[32,1024,16]{1,2,0:T(8,128)S(1)} %bitcast.138, f32[32,16,1024]{2,1,0:T(8,128)S(1)} %copy.59, pred[16,16]{1,0:T(8,128)(4,1)S(1)} %iota_compare_fusion.1), kind=kLoop, calls=%fused_computation.1 | loop fusion | flops 41418752 | bytes 6291712
  140.5 1.2 copy.122
  142.5 4.1 %copy.64 = f32[32,16,1024]{2,1,0:T(8,128)} copy(f32[32,16,1024]{2,0,1:T(8,128)} %get-tuple-element.11) | data formatting | bytes 4194304 | tf_op jit(solution)/shard_map/sub | solution.py:40
  146.6 0.2 slice.761
  146.8 0.2 slice.792
  147.8 0.5 slice.794
  148.2 3.7 %multiply_add_fusion = f32[32,16,1024]{2,0,1:T(8,128)S(1)} fusion(f32[32,1024]{1,0:T(8,128)S(1)} %concatenate.110, f32[32,1024,16]{1,2,0:T(8,128)} %copy-done.3, f32[32,16,1024]{2,0,1:T(8,128)} %get-tuple-element.10), kind=kLoop, calls=%fused_computation.39 | loop fusion | flops 1048576 | bytes 6422528 | tf_op jit(solution)/shard_map/add | solution.py:62
  152.0 1.2 copy.68
  153.2 1.4 copy-done.6
  154.6 0.2 slice.763
  154.9 2.8 %bitcast_multiply_fusion.2 = f32[512,1024]{1,0:T(8,128)S(1)} fusion(f32[32,16,1024]{2,1,0:T(8,128)} %copy.64, f32[32,1024]{1,0:T(8,128)S(1)} %concatenate.105, f32[512,2,1024]{2,0,1:T(8,128)} %copy-done.1), kind=kLoop, calls=%fused_computation.32 | loop fusion | flops 1048576 | bytes 6422528 | tf_op jit(solution)/shard_map/mul | solution.py:61
  157.7 1.4 copy-done.5
  159.9 3.7 %broadcast_multiply_fusion = (f32[32,16,1024]{2,0,1:T(8,128)S(1)}, f32[32,16,1024]{2,0,1:T(8,128)S(1)}) fusion(f32[32,1024]{1,0:T(8,128)S(1)} %concatenate.100, f32[32,16,1024]{2,0,1:T(8,128)} %get-tuple-element.97, f32[32,1024]{1,0:T(8,128)S(1)} %concatenate.95, f32[32,1024,16]{1,2,0:T(8,128)} %copy-done.4), kind=kLoop, calls=%fused_computation.62 | loop fusion | flops 1572864 | bytes 8650752 | tf_op jit(solution)/shard_map/mul | solution.py:61
  163.6 1.2 copy.62
  164.9 1.2 copy.61
  166.2 1.4 copy-done.8
  167.6 24.5 %all-gather.1 = f32[16,4,1024]{2,1,0:T(4,128)S(1)} all-gather(f32[1,4,1024]{2,1,0:T(4,128)S(1)} %maximum_bitcast_fusion), channel_id=2, replica_groups=mesh['sp'=16,'tp'=2] {'sp'}, dimensions={0}, use_global_device_ids=true | all-gather | bytes 278528 | tf_op jit(solution)/shard_map/all_gather | solution.py:134
  192.1 0.2 fusion.80
  193.1 0.4 slice.835
  193.8 0.2 slice.832
  194.6 0.2 slice.861
  194.8 0.2 slice.830
  195.3 0.2 rev.2
  195.6 13.8 %fusion.28 = f32[512,2048]{1,0:T(8,128)} fusion(bf16[1024,2048]{1,0:T(8,128)(2,1)} %param.26, f32[512,1024]{1,0:T(8,128)} %copy-done.5, f32[512,1024]{1,0:T(8,128)} %bitcast.133, f32[512,1024]{1,0:T(8,128)} %bitcast.137, f32[512,1024]{1,0:T(8,128)} %bitcast.135, bf16[2048,1024]{1,0:T(8,128)(2,1)} %param.17, f32[1024]{0:T(1024)S(1)} %bitcast.157, ...), kind=kOutput, calls=%fused_computation.63 | convolution fusion | flops 4308074496 | bytes 23087104 | tf_op jit(solution)/shard_map/dot_general | solution.py:29
  210.0 0.3 fusion.77
  210.3 0.6 copy-done.19
  210.9 1.3 fusion.29
  212.3 0.8 copy-done.2
  213.1 2.6 %add_convert_fusion = bf16[512,2048]{1,0:T(8,128)(2,1)} fusion(f32[512,2048]{1,0:T(8,128)S(1)} %copy-done.2, bf16[512,512]{0,1:T(8,128)(2,1)S(1)} %fusion.27, bf16[512,2048]{1,0:T(8,128)(2,1)S(1)} %copy-done), kind=kOutput, calls=%fused_computation.12 | convolution fusion | flops 1075838976 | bytes 8912896 | tf_op jit(solution)/shard_map/dot_general | solution.py:29
  215.7 28.4 %reduce-scatter.2.cloned.1.call-done = bf16[256,2048]{1,0:T(8,128)(2,1)} async-done(((bf16[512,2048]{1,0:T(8,128)(2,1)}), bf16[256,2048]{1,0:T(8,128)(2,1)}) %reduce-scatter.2.cloned.1.call-update) | async-done | bytes 1048592 | tf_op jit(solution)/shard_map/reduce_scatter | solution.py:183
  (297 shorter events, 5.5 us)
Async XLA Ops:
  6.5 205.8 %copy-start = (bf16[512,2048]{1,0:T(8,128)(2,1)S(1)}, bf16[512,2048]{1,0:T(8,128)(2,1)}, u32[]{:S(2)}) copy-start(bf16[512,2048]{1,0:T(8,128)(2,1)} %param.27) | copy-start | bytes 6291460
  6.5 3.9 %copy-start.16 = (f32[2,512]{1,0:T(2,128)S(1)}, f32[2,512]{1,0:T(2,128)}, u32[]{:S(2)}) copy-start(f32[2,512]{1,0:T(2,128)} %param.22) | copy-start | bytes 12292
  6.5 3.9 %copy-start.15 = (f32[2,1024]{1,0:T(2,128)S(1)}, f32[2,1024]{1,0:T(2,128)}, u32[]{:S(2)}) copy-start(f32[2,1024]{1,0:T(2,128)} %param.21) | copy-start | bytes 24580
  6.5 3.9 %copy-start.14 = (bf16[4,1024]{1,0:T(4,128)(2,1)S(1)}, bf16[4,1024]{1,0:T(4,128)(2,1)}, u32[]{:S(2)}) copy-start(bf16[4,1024]{1,0:T(4,128)(2,1)} %param.19) | copy-start | bytes 24580
  6.5 38.2 %all-gather.4.cloned.1.call-start = ((), (), s32[]{:S(2)}) async-start(), calls=%async_computation.1 | async-start | bytes 3145728 | tf_op jit(solution)/shard_map/all_gather | solution.py:85
  7.3 236.9 %reduce-scatter.2.cloned.1.call-start = ((), (), s32[]{:S(2)}) async-start(), calls=%async_computation.2 | async-start | bytes 3145728 | tf_op jit(solution)/shard_map/reduce_scatter | solution.py:183
  44.7 2.2 copy-start.9
  47.0 7.6 %copy-start.18 = (bf16[2048,512]{1,0:T(8,128)(2,1)S(1)}, bf16[2048,512]{1,0:T(8,128)(2,1)}, u32[]{:S(2)}) copy-start(bf16[2048,512]{1,0:T(8,128)(2,1)} %param.18) | copy-start | bytes 6291460
  51.8 10.0 %collective-permute-start = (bf16[2,1024]{1,0:T(2,128)(2,1)S(1)}, bf16[2,1024]{1,0:T(2,128)(2,1)S(1)}, u32[]{:S(2)}, u32[]{:S(2)}) collective-permute-start(bf16[2,1024]{1,0:T(2,128)(2,1)S(1)} %get-tuple-element.22), channel_id=1, source_target_pairs={{0,2},{2,4},{4,6},{6,8},{8,10},{10,12},{12,14},{14,16},{16,18},{18... | collective-permute-start | bytes 12296 | tf_op jit(solution)/shard_map/ppermute | solution.py:16
  53.3 8.4 %collective-permute-start.1 = (bf16[2,1024]{1,0:T(2,128)(2,1)S(1)}, bf16[2,1024]{1,0:T(2,128)(2,1)S(1)}, u32[]{:S(2)}, u32[]{:S(2)}) collective-permute-start(bf16[2,1024]{1,0:T(2,128)(2,1)S(1)} %get-tuple-element.23), channel_id=1, source_target_pairs={{2,0},{4,2},{6,4},{8,6},{10,8},{12,10},{14,12},{16,14},{18,16},{20... | collective-permute-start | bytes 12296 | tf_op jit(solution)/shard_map/ppermute | solution.py:19
  55.9 6.1 %copy-start.12 = (bf16[512,512]{1,0:T(8,128)(2,1)}, bf16[512,512]{1,0:T(8,128)(2,1)S(1)}, u32[]{:S(2)}) copy-start(bf16[512,512]{1,0:T(8,128)(2,1)S(1)} %convolution_convert_fusion.2) | copy-start | bytes 1572868
  56.0 153.4 %collective-permute-start.2 = (bf16[8,512]{1,0:T(8,128)(2,1)S(1)}, bf16[8,512]{1,0:T(8,128)(2,1)S(1)}, u32[]{:S(2)}, u32[]{:S(2)}) collective-permute-start(bf16[8,512]{1,0:T(8,128)(2,1)S(1)} %get-tuple-element.24), channel_id=1, source_target_pairs={{0,2},{2,4},{4,6},{6,8},{8,10},{10,12},{12,14},{14,16},{16,18},{18... | collective-permute-start | bytes 24584 | tf_op jit(solution)/shard_map/ppermute | solution.py:16
  60.4 148.9 %collective-permute-start.3 = (bf16[8,512]{1,0:T(8,128)(2,1)S(1)}, bf16[8,512]{1,0:T(8,128)(2,1)S(1)}, u32[]{:S(2)}, u32[]{:S(2)}) collective-permute-start(bf16[8,512]{1,0:T(8,128)(2,1)S(1)} %get-tuple-element.25), channel_id=1, source_target_pairs={{2,0},{4,2},{6,4},{8,6},{10,8},{12,10},{14,12},{16,14},{18,16},{20... | collective-permute-start | bytes 24584 | tf_op jit(solution)/shard_map/ppermute | solution.py:19
  81.3 5.4 %copy-start.17 = (f32[2,512]{1,0:T(2,128)S(1)}, f32[2,512]{1,0:T(2,128)}, u32[]{:S(2)}) copy-start(f32[2,512]{1,0:T(2,128)} %param.23) | copy-start | bytes 12292
  94.0 3.9 %copy-start.1 = (f32[512,2,1024]{2,0,1:T(8,128)}, f32[512,2,1024]{2,0,1:T(8,128)S(1)}, u32[]{:S(2)}) copy-start(f32[512,2,1024]{2,0,1:T(8,128)S(1)} %get-tuple-element.6) | copy-start | bytes 12582916
  102.9 3.0 %copy-start.11 = (f32[512,1,1024]{2,0,1:T(8,128)S(1)}, f32[512,1,1024]{2,0,1:T(8,128)}, u32[]{:S(2)}) copy-start(f32[512,1,1024]{2,0,1:T(8,128)} %get-tuple-element.98) | copy-start | bytes 6291460
  118.2 1.3 copy-start.3
  125.3 3.0 %copy-start.10 = (f32[512,1,1024]{2,0,1:T(8,128)S(1)}, f32[512,1,1024]{2,0,1:T(8,128)}, u32[]{:S(2)}) copy-start(f32[512,1,1024]{2,0,1:T(8,128)} %get-tuple-element.99) | copy-start | bytes 6291460
  140.4 1.3 copy-start.4
  153.2 1.4 copy-start.6
  157.7 1.4 copy-start.5
  164.9 1.3 copy-start.7
  166.2 1.4 copy-start.8
  195.6 13.8 %copy-start.13 = (bf16[512,512]{1,0:T(8,128)(2,1)S(1)}, bf16[512,512]{1,0:T(8,128)(2,1)}, u32[]{:S(2)}) copy-start(bf16[512,512]{1,0:T(8,128)(2,1)} %copy-done.12) | copy-start | bytes 1572868
  210.0 0.9 copy-start.19
  210.9 2.2 copy-start.2
Sparse Core Ops, SparseCore 0:
  8.9 35.8 all-gather.3
  215.9 28.2 reduce-scatter.1
where the time goes:
time: 256 us; the launch traced here: 251 us
  waiting for transfers between devices  63.3 us (25%)
  other arithmetic  59.5 us (23%)
  local copies, waits for them, and re-layouts  53.5 us (21%)
  matrix products  26.1 us (10%)
  blocking collectives  24.5 us (10%)
  between operations  15.5 us (6%)
  starting transfers between devices  8.69 us (3%)
    all_gather x1, waiting for transfers between devices, local(): lax.all_gather(incoming_activity, 'tp', axis=0, tiled=True)  34.2 us
    reduce_scatter x1, waiting for transfers between devices, local(): lax.psum_scatter((product(state_mix, recursive_final_matrix) + product(po...  28.4 us
    all_gather x1, blocking collectives, local(): totals = lax.all_gather(summary, 'sp', axis=0, tiled=True)  24.5 us
    unnamed x3, other arithmetic  24.5 us
    dot_general x4, matrix products, product(): return jnp.dot(left, right, preferred_element_type=jnp.float32)  22.4 us
    unnamed x51, local copies, waits for them, and re-layouts  18.9 us
    mul x1, other arithmetic, local(): jnp.sqrt(-jnp.expm1(2.0 * logarithmic_persistence)) * inlet  7.26 us
    mul x2, other arithmetic, block_chain(): keep_all = decay * prior_keep[:, None]  6.51 us
  transfers between devices with their start and end apart: 6, of which 2 were waited for; matrix products, arithmetic and copies ran while one was open for 48% of the time, Pallas kernels for 0%

commit v1 on v0

--- a/solution.py
+++ b/solution.py
@@ -131,7 +131,15 @@
     summary = jnp.stack([forward_keep[-1], forward_local[-1], backward_keep[0], backward_local[0]])[
         None
     ]
-    totals = lax.all_gather(summary, "sp", axis=0, tiled=True)
+    ways, here = (lax.axis_size("sp"), lax.axis_index("sp"))
+    grown, reach = (summary, 1)
+    while reach < ways:
+        theirs = lax.ppermute(grown, "sp", [(d, d ^ reach) for d in range(ways)])
+        mine_first = jnp.concatenate([grown, theirs], axis=0)
+        theirs_first = jnp.concatenate([theirs, grown], axis=0)
+        grown = jnp.where(here & reach == 0, mine_first, theirs_first)
+        reach = 2 * reach
+    totals = grown
     place = lax.axis_index("sp")
     forward_all = lax.associative_scan(combine, (totals[:, 0], totals[:, 1]), axis=0)
     backward_all = lax.associative_scan(combine, (totals[:, 2], totals[:, 3]), axis=0, reverse=True)

time: 256 us -> 253 us (0.988)
  blocking collectives: 24.5 us -> 0 us
  starting transfers between devices: 8.69 us -> 20.1 us
  waiting for transfers between devices: 63.3 us -> 73.9 us
  local copies, waits for them, and re-layouts: 53.5 us -> 50.8 us
    all_gather x1 -> x0, blocking collectives: 24.5 us -> none  [local(): totals = lax.all_gather(summary, 'sp', axis=0, tiled=True)]
    ppermute x0 -> x4, starting transfers between devices: none -> 11.4 us  [local(): theirs = lax.ppermute(grown, 'sp', [(d, d ^ reach) for d in range(ways)])]
    ppermute x0 -> x4, waiting for transfers between devices: none -> 5.96 us  [local(): theirs = lax.ppermute(grown, 'sp', [(d, d ^ reach) for d in range(ways)])]
    reduce_scatter x1, waiting for transfers between devices: 28.4 us -> 33 us  [local(): lax.psum_scatter((product(state_mix, recursive_final_matrix) + product(po...]
    unnamed x51 -> x49, local copies, waits for them, and re-layouts: 18.9 us -> 16.2 us
    unnamed x3 -> x2, other arithmetic: 24.5 us -> 24.4 us
  transfers between devices with their start and end apart: 6 -> 10, of which waited for: 2 -> 6; matrix products, arithmetic and copies ran while one was open for 48% -> 43% of each run, Pallas kernels for 0% -> 0%
where the time goes in v1:
time: 253 us; the launch traced here: 248 us
  waiting for transfers between devices  73.9 us (29%)
  other arithmetic  59.6 us (24%)
  local copies, waits for them, and re-layouts  50.8 us (20%)
  matrix products  28.3 us (11%)
  starting transfers between devices  20.1 us (8%)
  between operations  15.5 us (6%)
    all_gather x1, waiting for transfers between devices, local(): lax.all_gather(incoming_activity, 'tp', axis=0, tiled=True)  34.2 us
    reduce_scatter x1, waiting for transfers between devices, local(): lax.psum_scatter((product(state_mix, recursive_final_matrix) + product(po...  33 us
    dot_general x4, matrix products, product(): return jnp.dot(left, right, preferred_element_type=jnp.float32)  24.6 us
    unnamed x2, other arithmetic  24.4 us
    unnamed x49, local copies, waits for them, and re-layouts  16.2 us
    ppermute x4, starting transfers between devices, local(): theirs = lax.ppermute(grown, 'sp', [(d, d ^ reach) for d in range(ways)])  11.4 us
    mul x1, other arithmetic, local(): jnp.sqrt(-jnp.expm1(2.0 * logarithmic_persistence)) * inlet  7.26 us
    mul x2, other arithmetic, block_chain(): keep_all = decay * prior_keep[:, None]  6.51 us
  transfers between devices with their start and end apart: 10, of which 6 were waited for; matrix products, arithmetic and copies ran while one was open for 43% of the time, Pallas kernels for 0%

profile of v1, /device:TPU:0, one launch (start us, length us, event | category | flops | bytes accessed | tf_op | source)
XLA Modules:
  0.0 248.2 jit_solution(4559328346790263488)
XLA Ops:
  6.6 0.7 all-gather.2.cloned.1.call-update
  7.3 0.7 convert_element_type.101
  8.0 0.7 convert_element_type.85
  8.7 1.6 copy.34
  10.5 34.2 %all-gather.2.cloned.1.call-done = bf16[512,2048]{1,0:T(8,128)(2,1)} async-done(((bf16[256,2048]{1,0:T(8,128)(2,1)}), bf16[512,2048]{1,0:T(8,128)(2,1)}) %all-gather.2.cloned.1.call-update) | async-done | bytes 2097168 | tf_op jit(solution)/shard_map/all_gather | solution.py:85
  44.7 2.2 fusion
  47.0 4.7 %convolution_convert_fusion = bf16[512,1024]{1,0:T(8,128)(2,1)S(1)} fusion(bf16[2048,1024]{1,0:T(8,128)(2,1)} %param.16, bf16[512,2048]{1,0:T(8,128)(2,1)S(1)} %copy-done.8, f32[2048]{0:T(1024)S(1)} %convert_element_type.85, f32[512]{0:T(512)S(1)} %add_rsqrt_fusion), kind=kOutput, calls=%fused_computation.44 | convolution fusion | flops 2152202240 | bytes 7350272 | tf_op jit(solution)/shard_map/dot_general | solution.py:29
  51.8 1.6 collective-permute-start
  53.3 1.3 collective-permute-start.1
  54.6 1.3 convolution_convert_fusion.2
  56.0 4.5 %collective-permute-start.6 = (bf16[8,512]{1,0:T(8,128)(2,1)S(1)}, bf16[8,512]{1,0:T(8,128)(2,1)S(1)}, u32[]{:S(2)}, u32[]{:S(2)}) collective-permute-start(bf16[8,512]{1,0:T(8,128)(2,1)S(1)} %get-tuple-element.24), channel_id=1, source_target_pairs={{0,2},{2,4},{4,6},{6,8},{8,10},{10,12},{12,14},{14,16},{16,18},{18... | collective-permute-start | bytes 24584 | tf_op jit(solution)/shard_map/ppermute | solution.py:16
  60.4 1.3 collective-permute-start.7
  61.8 0.3 maximum_convert_fusion
  62.1 2.6 %fusion.71 = (f32[512,1024]{1,0:T(8,128)}, bf16[512,1024]{1,0:T(8,128)(2,1)}) fusion(f32[516,1024]{1,0:T(8,128)S(1)} %maximum_convert_fusion, f32[1024]{0:T(1024)S(1)} %bitcast.154, f32[1024]{0:T(1024)S(1)} %bitcast.155, f32[1024]{0:T(1024)S(1)} %bitcast.153, f32[1024]{0:T(1024)S(1)} %bitcast.152), kind=kLoop, calls=%fused_computation.231 | loop fusion | flops 4718592 | bytes 11550720 | tf_op jit(solution)/shard_map/convert_element_type | solution.py:108
  64.7 2.8 %copy.33 = bf16[512,1024]{0,1:T(8,128)(2,1)} copy(bf16[512,1024]{1,0:T(8,128)(2,1)} %get-tuple-element.8) | data formatting | bytes 2097152 | tf_op jit(solution)/shard_map/convert_element_type | solution.py:107
  67.5 2.4 fusion.96
  69.9 1.8 copy.35
  71.7 4.2 %fusion.74 = (f32[512,2,1,1024]{0,3,2,1:T(8,128)}, f32[512,2,1,1024]{0,3,2,1:T(8,128)}) fusion(f32[512,2,2,1024]{0,3,2,1:T(8,128)S(1)} %bitcast.122), kind=kLoop, calls=%fused_computation.233 | loop fusion | bytes 16777216 | tf_op jit(solution)/shard_map/slice | solution.py:117
  75.9 5.4 %copy.72 = f32[512,2,1,1024]{3,0,1,2:T(8,128)} copy(f32[512,2,1,1024]{0,3,2,1:T(8,128)} %get-tuple-element.12) | data formatting | bytes 8388608
  81.3 5.4 %copy.73 = f32[512,2,1,1024]{3,0,1,2:T(8,128)} copy(f32[512,2,1,1024]{0,3,2,1:T(8,128)} %get-tuple-element.13) | data formatting | bytes 8388608
  86.7 7.3 %fusion.3 = (f32[512,2,1024]{2,0,1:T(8,128)S(1)}, f32[512,2,1024]{2,0,1:T(8,128)S(1)}) fusion(f32[512,2,1,1024]{3,0,1,2:T(8,128)} %copy.73, f32[512,1024]{1,0:T(8,128)} %get-tuple-element.7, f32[512,2]{0,1:T(2,128)S(1)} %bitcast.158, f32[2,1024]{1,0:T(2,128)S(1)} %compare_select_fusion, f32[512,2,1,1024]{3,0,1,2:T(8,128)} %copy.72, ...), kind=kLoop, calls=%fused_computation.8 | loop fusion | flops 13631488 | bytes 18890752 | tf_op jit(solution)/shard_map/mul | solution.py:127
  94.0 3.3 %fusion.75 = (f32[512,1,1024]{2,0,1:T(8,128)}, f32[512,1,1024]{2,0,1:T(8,128)S(1)}, f32[512,1,1024]{2,0,1:T(8,128)}, f32[512,1,1024]{2,0,1:T(8,128)}) fusion(f32[512,2,1024]{2,0,1:T(8,128)S(1)} %get-tuple-element.6, f32[512,2,1024]{2,0,1:T(8,128)S(1)} %get-tuple-element.5), kind=kLoop, calls=%fused_computation.234 | loop fusion | bytes 16777216 | tf_op jit(solution)/shard_map/slice | solution.py:128
  97.3 0.6 copy-done.1
  97.9 1.3 fusion.20
  99.2 3.6 %fusion.73 = (f32[32,16,1024]{2,0,1:T(8,128)S(1)}, f32[32,16,1024]{2,0,1:T(8,128)}, f32[32,16,1024]{2,0,1:T(8,128)}) fusion(f32[32,16,1024]{2,1,0:T(8,128)S(1)} %bitcast.124, f32[32,16,1024]{2,0,1:T(8,128)S(1)} %fusion.20, f32[32,1024]{1,0:T(8,128)S(1)} %slice_bitcast_fusion.2), kind=kLoop, calls=%fused_computation.232 | loop fusion | flops 1048576 | bytes 10616832 | tf_op jit(solution)/shard_map/exp | solution.py:48
  102.9 3.0 %copy.46 = f32[32,16,1024]{2,1,0:T(8,128)S(1)} copy(f32[32,16,1024]{2,0,1:T(8,128)} %get-tuple-element.10) | data formatting | bytes 4194304 | tf_op jit(solution)/shard_map/add | solution.py:40
  105.9 12.3 %multiply_reduce_fusion = f32[32,1024,16]{1,2,0:T(8,128)S(1)} fusion(f32[32,1024,16]{1,2,0:T(8,128)S(1)} %bitcast.139, f32[32,16,1024]{2,1,0:T(8,128)S(1)} %copy.46, pred[16,16]{1,0:T(8,128)(4,1)S(1)} %iota_compare_fusion), kind=kLoop, calls=%fused_computation | loop fusion | flops 41418752 | bytes 6291712
  118.2 1.2 copy.101
  119.6 0.2 slice.739
  119.8 0.2 slice.741
  120.0 0.2 slice.770
  120.9 4.3 %fusion.95 = (f32[32,16,1024]{2,0,1:T(8,128)S(1)}, f32[32,16,1024]{2,0,1:T(8,128)}) fusion(f32[32,16,1024]{2,1,0:T(8,128)} %bitcast.125), kind=kOutput, calls=%fused_computation.254 | output fusion | flops 7864320 | bytes 6291456 | tf_op jit(solution)/shard_map/jit(cumsum)/reduce_window_sum | solution.py:37
  125.3 3.0 %copy.39 = f32[32,16,1024]{2,1,0:T(8,128)S(1)} copy(f32[32,16,1024]{2,0,1:T(8,128)} %get-tuple-element.97) | data formatting | bytes 4194304 | tf_op jit(solution)/shard_map/jit(cumsum)/reduce_window_sum | solution.py:37
  128.3 12.1 %multiply_reduce_fusion.1 = f32[32,1024,16]{1,2,0:T(8,128)S(1)} fusion(f32[32,1024,16]{1,2,0:T(8,128)S(1)} %bitcast.138, f32[32,16,1024]{2,1,0:T(8,128)S(1)} %copy.39, pred[16,16]{1,0:T(8,128)(4,1)S(1)} %iota_compare_fusion.1), kind=kLoop, calls=%fused_computation.1 | loop fusion | flops 41418752 | bytes 6291712
  140.5 1.2 copy.102
  142.5 4.1 %copy.44 = f32[32,16,1024]{2,1,0:T(8,128)} copy(f32[32,16,1024]{2,0,1:T(8,128)} %get-tuple-element.11) | data formatting | bytes 4194304 | tf_op jit(solution)/shard_map/sub | solution.py:40
  146.6 0.2 slice.761
  146.8 0.2 slice.792
  147.8 0.5 slice.794
  148.3 3.7 %multiply_add_fusion = f32[32,16,1024]{2,0,1:T(8,128)S(1)} fusion(f32[32,1024]{1,0:T(8,128)S(1)} %concatenate.134, f32[32,1024,16]{1,2,0:T(8,128)} %copy-done.2, f32[32,16,1024]{2,0,1:T(8,128)} %get-tuple-element.10), kind=kLoop, calls=%fused_computation.39 | loop fusion | flops 1048576 | bytes 6422528 | tf_op jit(solution)/shard_map/add | solution.py:62
  152.0 1.2 copy.48
  153.2 1.4 copy-done.5
  154.6 0.2 slice.763
  154.9 2.8 %bitcast_multiply_fusion.2 = f32[512,1024]{1,0:T(8,128)S(1)} fusion(f32[32,16,1024]{2,1,0:T(8,128)} %copy.44, f32[32,1024]{1,0:T(8,128)S(1)} %concatenate.129, f32[512,2,1024]{2,0,1:T(8,128)} %copy-done.1), kind=kLoop, calls=%fused_computation.32 | loop fusion | flops 1048576 | bytes 6422528 | tf_op jit(solution)/shard_map/mul | solution.py:61
  157.7 1.4 copy-done.4
  159.9 3.7 %broadcast_multiply_fusion = (f32[32,16,1024]{2,0,1:T(8,128)S(1)}, f32[32,16,1024]{2,0,1:T(8,128)S(1)}) fusion(f32[32,1024]{1,0:T(8,128)S(1)} %concatenate.124, f32[32,16,1024]{2,0,1:T(8,128)} %get-tuple-element.97, f32[32,1024]{1,0:T(8,128)S(1)} %concatenate.119, f32[32,1024,16]{1,2,0:T(8,128)} %copy-done.3), kind=kLoop, calls=%fused_computation.62 | loop fusion | flops 1572864 | bytes 8650752 | tf_op jit(solution)/shard_map/mul | solution.py:61
  163.6 1.2 copy.42
  164.9 1.2 copy.41
  166.2 2.4 collective-permute-start.2
  169.2 0.2 collective-permute-done.2
  169.5 2.4 collective-permute-start.3
  171.9 0.3 fusion.77
  172.2 1.9 collective-permute-done.3
  174.2 3.6 %collective-permute-start.4 = (f32[4,4,1024]{2,1,0:T(4,128)S(1)}, f32[4,4,1024]{2,1,0:T(4,128)S(1)}, u32[]{:S(2)}, u32[]{:S(2)}) collective-permute-start(f32[4,4,1024]{2,1,0:T(4,128)S(1)} %maximum_select_fusion.2), channel_id=1, source_target_pairs={{0,8},{2,10},{4,12},{6,14},{8,0},{10,2},{12,4},{14,6},{16,24},{18,... | collective-permute-start | bytes 196616 | tf_op jit(solution)/shard_map/ppermute | solution.py:137
  177.7 1.2 fusion.29
  179.0 1.0 collective-permute-done.4
  180.0 3.0 %collective-permute-start.5 = (f32[8,4,1024]{2,1,0:T(4,128)S(1)}, f32[8,4,1024]{2,1,0:T(4,128)S(1)}, u32[]{:S(2)}, u32[]{:S(2)}) collective-permute-start(f32[8,4,1024]{2,1,0:T(4,128)S(1)} %maximum_select_fusion.1), channel_id=1, source_target_pairs={{0,16},{2,18},{4,20},{6,22},{8,24},{10,26},{12,28},{14,30},{16,0},... | collective-permute-start | bytes 393224 | tf_op jit(solution)/shard_map/ppermute | solution.py:137
  183.2 2.8 %collective-permute-done.5 = f32[8,4,1024]{2,1,0:T(4,128)S(1)} collective-permute-done((f32[8,4,1024]{2,1,0:T(4,128)S(1)}, f32[8,4,1024]{2,1,0:T(4,128)S(1)}, u32[]{:S(2)}, u32[]{:S(2)}) %collective-permute-start.5) | collective-permute-done | bytes 131104 | tf_op jit(solution)/shard_map/ppermute | solution.py:137
  186.1 0.2 fusion.80
  188.0 0.5 slice.861
  188.8 0.2 slice.830
  189.5 13.7 %fusion.28 = f32[512,2048]{1,0:T(8,128)} fusion(bf16[1024,2048]{1,0:T(8,128)(2,1)} %param.26, f32[512,1024]{1,0:T(8,128)} %copy-done.4, f32[512,1024]{1,0:T(8,128)} %bitcast.133, f32[512,1024]{1,0:T(8,128)} %bitcast.137, f32[512,1024]{1,0:T(8,128)} %bitcast.135, bf16[2048,1024]{1,0:T(8,128)(2,1)} %param.17, f32[1024]{0:T(1024)S(1)} %bitcast.157, ...), kind=kOutput, calls=%fused_computation.63 | convolution fusion | flops 4308074496 | bytes 23087104 | tf_op jit(solution)/shard_map/dot_general | solution.py:29
  203.2 4.8 %add_convert_fusion = bf16[512,2048]{1,0:T(8,128)(2,1)} fusion(f32[512,2048]{1,0:T(8,128)} %fusion.28, bf16[512,512]{0,1:T(8,128)(2,1)S(1)} %fusion.27, bf16[512,2048]{1,0:T(8,128)(2,1)S(1)} %copy-done), kind=kOutput, calls=%fused_computation.12 | convolution fusion | flops 1075838976 | bytes 8912896 | tf_op jit(solution)/shard_map/dot_general | solution.py:29
  208.1 33.0 %reduce-scatter.2.cloned.1.call-done = bf16[256,2048]{1,0:T(8,128)(2,1)} async-done(((bf16[512,2048]{1,0:T(8,128)(2,1)}), bf16[256,2048]{1,0:T(8,128)(2,1)}) %reduce-scatter.2.cloned.1.call-update) | async-done | bytes 1048592 | tf_op jit(solution)/shard_map/reduce_scatter | solution.py:191
  (306 shorter events, 6.2 us)
Async XLA Ops:
  6.5 196.7 %copy-start = (bf16[512,2048]{1,0:T(8,128)(2,1)S(1)}, bf16[512,2048]{1,0:T(8,128)(2,1)}, u32[]{:S(2)}) copy-start(bf16[512,2048]{1,0:T(8,128)(2,1)} %param.27) | copy-start | bytes 6291460
  6.5 3.9 %copy-start.15 = (f32[2,512]{1,0:T(2,128)S(1)}, f32[2,512]{1,0:T(2,128)}, u32[]{:S(2)}) copy-start(f32[2,512]{1,0:T(2,128)} %param.22) | copy-start | bytes 12292
  6.5 3.9 %copy-start.14 = (f32[2,1024]{1,0:T(2,128)S(1)}, f32[2,1024]{1,0:T(2,128)}, u32[]{:S(2)}) copy-start(f32[2,1024]{1,0:T(2,128)} %param.21) | copy-start | bytes 24580
  6.5 4.0 %copy-start.13 = (bf16[4,1024]{1,0:T(4,128)(2,1)S(1)}, bf16[4,1024]{1,0:T(4,128)(2,1)}, u32[]{:S(2)}) copy-start(bf16[4,1024]{1,0:T(4,128)(2,1)} %param.19) | copy-start | bytes 24580
  6.5 38.2 %all-gather.2.cloned.1.call-start = ((), (), s32[]{:S(2)}) async-start(), calls=%async_computation.1 | async-start | bytes 3145728 | tf_op jit(solution)/shard_map/all_gather | solution.py:85
  7.3 233.9 %reduce-scatter.2.cloned.1.call-start = ((), (), s32[]{:S(2)}) async-start(), calls=%async_computation.2 | async-start | bytes 3145728 | tf_op jit(solution)/shard_map/reduce_scatter | solution.py:191
  44.7 2.2 copy-start.8
  47.0 7.6 %copy-start.17 = (bf16[2048,512]{1,0:T(8,128)(2,1)S(1)}, bf16[2048,512]{1,0:T(8,128)(2,1)}, u32[]{:S(2)}) copy-start(bf16[2048,512]{1,0:T(8,128)(2,1)} %param.18) | copy-start | bytes 6291460
  51.8 10.0 %collective-permute-start = (bf16[2,1024]{1,0:T(2,128)(2,1)S(1)}, bf16[2,1024]{1,0:T(2,128)(2,1)S(1)}, u32[]{:S(2)}, u32[]{:S(2)}) collective-permute-start(bf16[2,1024]{1,0:T(2,128)(2,1)S(1)} %get-tuple-element.22), channel_id=1, source_target_pairs={{0,2},{2,4},{4,6},{6,8},{8,10},{10,12},{12,14},{14,16},{16,18},{18... | collective-permute-start | bytes 12296 | tf_op jit(solution)/shard_map/ppermute | solution.py:16
  53.3 8.4 %collective-permute-start.1 = (bf16[2,1024]{1,0:T(2,128)(2,1)S(1)}, bf16[2,1024]{1,0:T(2,128)(2,1)S(1)}, u32[]{:S(2)}, u32[]{:S(2)}) collective-permute-start(bf16[2,1024]{1,0:T(2,128)(2,1)S(1)} %get-tuple-element.23), channel_id=1, source_target_pairs={{2,0},{4,2},{6,4},{8,6},{10,8},{12,10},{14,12},{16,14},{18,16},{20... | collective-permute-start | bytes 12296 | tf_op jit(solution)/shard_map/ppermute | solution.py:19
  55.9 6.1 %copy-start.11 = (bf16[512,512]{1,0:T(8,128)(2,1)}, bf16[512,512]{1,0:T(8,128)(2,1)S(1)}, u32[]{:S(2)}) copy-start(bf16[512,512]{1,0:T(8,128)(2,1)S(1)} %convolution_convert_fusion.2) | copy-start | bytes 1572868
  56.0 112.7 %collective-permute-start.6 = (bf16[8,512]{1,0:T(8,128)(2,1)S(1)}, bf16[8,512]{1,0:T(8,128)(2,1)S(1)}, u32[]{:S(2)}, u32[]{:S(2)}) collective-permute-start(bf16[8,512]{1,0:T(8,128)(2,1)S(1)} %get-tuple-element.24), channel_id=1, source_target_pairs={{0,2},{2,4},{4,6},{6,8},{8,10},{10,12},{12,14},{14,16},{16,18},{18... | collective-permute-start | bytes 24584 | tf_op jit(solution)/shard_map/ppermute | solution.py:16
  60.4 108.2 %collective-permute-start.7 = (bf16[8,512]{1,0:T(8,128)(2,1)S(1)}, bf16[8,512]{1,0:T(8,128)(2,1)S(1)}, u32[]{:S(2)}, u32[]{:S(2)}) collective-permute-start(bf16[8,512]{1,0:T(8,128)(2,1)S(1)} %get-tuple-element.25), channel_id=1, source_target_pairs={{2,0},{4,2},{6,4},{8,6},{10,8},{12,10},{14,12},{16,14},{18,16},{20... | collective-permute-start | bytes 24584 | tf_op jit(solution)/shard_map/ppermute | solution.py:19
  81.3 5.4 %copy-start.16 = (f32[2,512]{1,0:T(2,128)S(1)}, f32[2,512]{1,0:T(2,128)}, u32[]{:S(2)}) copy-start(f32[2,512]{1,0:T(2,128)} %param.23) | copy-start | bytes 12292
  94.0 3.9 %copy-start.1 = (f32[512,2,1024]{2,0,1:T(8,128)}, f32[512,2,1024]{2,0,1:T(8,128)S(1)}, u32[]{:S(2)}) copy-start(f32[512,2,1024]{2,0,1:T(8,128)S(1)} %get-tuple-element.6) | copy-start | bytes 12582916
  102.9 3.0 %copy-start.10 = (f32[512,1,1024]{2,0,1:T(8,128)S(1)}, f32[512,1,1024]{2,0,1:T(8,128)}, u32[]{:S(2)}) copy-start(f32[512,1,1024]{2,0,1:T(8,128)} %get-tuple-element.98) | copy-start | bytes 6291460
  118.2 1.3 copy-start.2
  125.3 3.0 %copy-start.9 = (f32[512,1,1024]{2,0,1:T(8,128)S(1)}, f32[512,1,1024]{2,0,1:T(8,128)}, u32[]{:S(2)}) copy-start(f32[512,1,1024]{2,0,1:T(8,128)} %get-tuple-element.99) | copy-start | bytes 6291460
  140.4 1.3 copy-start.3
  153.2 1.4 copy-start.5
  157.7 1.4 copy-start.4
  164.8 1.3 copy-start.6
  164.9 3.8 %copy-start.12 = (bf16[512,512]{1,0:T(8,128)(2,1)S(1)}, bf16[512,512]{1,0:T(8,128)(2,1)}, u32[]{:S(2)}) copy-start(bf16[512,512]{1,0:T(8,128)(2,1)} %copy-done.11) | copy-start | bytes 1572868
  166.2 2.8 %copy-start.7 = (f32[32,16,1024]{2,1,0:T(8,128)}, f32[32,16,1024]{2,1,0:T(8,128)S(1)}, u32[]{:S(2)}) copy-start(f32[32,16,1024]{2,1,0:T(8,128)S(1)} %copy.41) | copy-start | bytes 6291460
  166.2 3.3 %collective-permute-start.2 = (f32[1,4,1024]{2,1,0:T(4,128)S(1)}, f32[1,4,1024]{2,1,0:T(4,128)S(1)}, u32[]{:S(2)}, u32[]{:S(2)}) collective-permute-start(f32[1,4,1024]{2,1,0:T(4,128)S(1)} %maximum_bitcast_fusion), channel_id=1, source_target_pairs={{0,2},{2,0},{4,6},{6,4},{8,10},{10,8},{12,14},{14,12},{16,18},{18,... | collective-permute-start | bytes 49160 | tf_op jit(solution)/shard_map/ppermute | solution.py:137
  169.5 8.2 %copy-start.18 = (bf16[4,128,128]{2,1,0:T(8,128)(2,1)S(1)}, bf16[4,128,128]{2,1,0:T(8,128)(2,1)}, u32[]{:S(2)}) copy-start(bf16[4,128,128]{2,1,0:T(8,128)(2,1)} %param.24) | copy-start | bytes 393220
  169.5 4.6 %collective-permute-start.3 = (f32[2,4,1024]{2,1,0:T(4,128)S(1)}, f32[2,4,1024]{2,1,0:T(4,128)S(1)}, u32[]{:S(2)}, u32[]{:S(2)}) collective-permute-start(f32[2,4,1024]{2,1,0:T(4,128)S(1)} %maximum_select_fusion.3), channel_id=1, source_target_pairs={{0,4},{2,6},{4,0},{6,2},{8,12},{10,14},{12,8},{14,10},{16,20},{18,... | collective-permute-start | bytes 98312 | tf_op jit(solution)/shard_map/ppermute | solution.py:137
  174.2 5.8 %collective-permute-start.4 = (f32[4,4,1024]{2,1,0:T(4,128)S(1)}, f32[4,4,1024]{2,1,0:T(4,128)S(1)}, u32[]{:S(2)}, u32[]{:S(2)}) collective-permute-start(f32[4,4,1024]{2,1,0:T(4,128)S(1)} %maximum_select_fusion.2), channel_id=1, source_target_pairs={{0,8},{2,10},{4,12},{6,14},{8,0},{10,2},{12,4},{14,6},{16,24},{18,... | collective-permute-start | bytes 196616 | tf_op jit(solution)/shard_map/ppermute | solution.py:137
  180.0 6.0 %collective-permute-start.5 = (f32[8,4,1024]{2,1,0:T(4,128)S(1)}, f32[8,4,1024]{2,1,0:T(4,128)S(1)}, u32[]{:S(2)}, u32[]{:S(2)}) collective-permute-start(f32[8,4,1024]{2,1,0:T(4,128)S(1)} %maximum_select_fusion.1), channel_id=1, source_target_pairs={{0,16},{2,18},{4,20},{6,22},{8,24},{10,26},{12,28},{14,30},{16,0},... | collective-permute-start | bytes 393224 | tf_op jit(solution)/shard_map/ppermute | solution.py:137
Sparse Core Ops, SparseCore 0:
  8.9 35.8 all-gather.1
  208.2 32.8 reduce-scatter.1
